TPU v7x, 32 devices: a whole 2x2x4 slice. The times are simulated.
32 devices in a mesh: sp: 8 (over z, x), tp: 4 (over y, core).
Axes of the slice: x: 2, y: 2, z: 4, core: 2. Of those that a mesh axis runs over, the one named last changes fastest.
Arguments:
- tokens: bfloat16 [1024, 1024], P('sp', 'tp'), may hold values from -6 to 6
- norm_gain: float32 [3, 1024], replicated, may hold values from 0.1 to 1.9
- w_query: bfloat16 [3, 1024, 1024], P(None, 'sp', 'tp'), may hold values from -0.1875 to 0.1875
- w_key: bfloat16 [3, 1024, 1024], P(None, 'sp', 'tp'), may hold values from -0.1875 to 0.1875
- w_value: bfloat16 [3, 1024, 1024], P(None, 'sp', 'tp'), may hold values from -0.1875 to 0.1875
- w_out: bfloat16 [3, 1024, 1024], P(None, 'tp', 'sp'), may hold values from -0.5625 to 0.5625
- offset_bias: float32 [3, 16, 8, 16], P(None, 'tp'), may hold values from -3 to 3
- documents: int32 [1024], P('sp'), may hold values from 0 to 7, never falling along the last dimension, each value on 1 to 256 neighbouring positions
Outputs:
- mixed: bfloat16 [1024, 1024], P('sp', 'tp')
Inputs may be any that keep to these rules, and one draw needn't show every extreme that they name: `documents`: document numbers never fall along the token order, start at 0, and each document has 1 to 256 tokens.
All inputs are finite; a program needn't handle non-finite values.
Results may differ from a plain program's by a relative error of at most 0.02.
Values may be sent and summed in bfloat16 or wider, within the bound.
A program may use at most 64 MiB of HBM per device.

v0:
```python
import jax
import jax.numpy as jnp
from jax import lax
from jax.sharding import PartitionSpec as P

HEAD_DIM = 64
WIN_ROWS = 8
WIN_COLS = 16
LAYERS = 3
GRID_W = 32
EPS = 1e-06


def with_halo(shard, sides, width, wrap):
    for axis, dim in sides:
        count, length = (lax.axis_size(axis), shard.shape[dim])
        up = [(i, (i + 1) % count) for i in range(count if wrap else count - 1)]
        down = [(j, i) for i, j in up]
        last = lax.slice_in_dim(shard, length - width, length, axis=dim)
        leading = lax.slice_in_dim(shard, 0, width, axis=dim)
        before = lax.ppermute(last, axis, up)
        after = lax.ppermute(leading, axis, down)
        shard = jnp.concatenate([before, shard, after], axis=dim)
    return shard


def rms_rows(stream, gain_row):
    values = stream.astype(jnp.float32)
    mean_sq = jnp.mean(values * values, axis=-1, keepdims=True)
    return (values * lax.rsqrt(mean_sq + EPS) * gain_row).astype(jnp.bfloat16)


def head_norm(heads_raw):
    values = heads_raw.astype(jnp.float32)
    mean_sq = jnp.mean(values * values, axis=-1, keepdims=True)
    return (values * lax.rsqrt(mean_sq + EPS)).astype(jnp.bfloat16)


def attend(queries, fringe, seg_own, seg_fringe, bias_layer):
    row_count, grid_width, head_count, head_width = queries.shape
    key_rows = jnp.stack(
        [fringe[row_lag : row_lag + row_count] for row_lag in range(WIN_ROWS)], axis=1
    )
    seg_rows = jnp.stack(
        [seg_fringe[row_lag : row_lag + row_count] for row_lag in range(WIN_ROWS)], axis=1
    )
    key_part = key_rows[..., :head_width]
    value_part = key_rows[..., head_width:]
    scores = jnp.einsum(
        "rchd,rjkhd->rhcjk", queries, key_part, preferred_element_type=jnp.float32
    ) * head_width ** (-0.5)
    column = jnp.arange(grid_width)
    col_offset = column[None, :] - column[:, None] + WIN_COLS // 2
    inside = (col_offset >= 0) & (col_offset < WIN_COLS)
    bias_table = bias_layer[:, :, jnp.clip(col_offset, 0, WIN_COLS - 1)]
    scores = scores + jnp.transpose(bias_table, (0, 2, 1, 3))[None]
    same_doc = seg_rows[:, None, None, :, :] == seg_own[:, None, :, None, None]
    allowed = same_doc & inside[None, None, :, None, :]
    scores = jnp.where(allowed, scores, -1e30)
    flat = scores.reshape(row_count, head_count, grid_width, WIN_ROWS * grid_width)
    attn_probs = jax.nn.softmax(flat, axis=-1).astype(jnp.bfloat16)
    attn_probs = attn_probs.reshape(row_count, head_count, grid_width, WIN_ROWS, grid_width)
    mixed_heads = jnp.einsum(
        "rhcjk,rjkhd->rchd", attn_probs, value_part, preferred_element_type=jnp.float32
    )
    return mixed_heads.astype(jnp.bfloat16)


def body(tokens, norm_gain, w_query, w_key, w_value, w_out, offset_bias, documents):
    token_count = tokens.shape[0]
    row_count = token_count // GRID_W
    reach_rows = WIN_ROWS // 2
    head_count = offset_bias.shape[1]
    seg_own = (documents + 1).reshape(row_count, GRID_W)
    seg_fringe = with_halo(seg_own, (("sp", 0),), reach_rows, False)
    collected = (
        lax.all_gather(w_query, "sp", axis=1, tiled=True),
        lax.all_gather(w_key, "sp", axis=1, tiled=True),
        lax.all_gather(w_value, "sp", axis=1, tiled=True),
        lax.all_gather(w_out, "sp", axis=2, tiled=True),
    )
    stream = tokens
    for layer_index in range(LAYERS):
        gathered = lax.all_gather(stream, "tp", axis=1, tiled=True)
        normed = rms_rows(gathered, norm_gain[layer_index])
        query_raw = jnp.dot(normed, collected[0][layer_index], preferred_element_type=jnp.float32)
        key_raw = jnp.dot(normed, collected[1][layer_index], preferred_element_type=jnp.float32)
        value_raw = jnp.dot(normed, collected[2][layer_index], preferred_element_type=jnp.float32)
        query_heads = head_norm(
            query_raw.astype(jnp.bfloat16).reshape(row_count, GRID_W, head_count, HEAD_DIM)
        )
        key_heads = head_norm(
            key_raw.astype(jnp.bfloat16).reshape(row_count, GRID_W, head_count, HEAD_DIM)
        )
        value_heads = value_raw.astype(jnp.bfloat16).reshape(
            row_count, GRID_W, head_count, HEAD_DIM
        )
        key_value = jnp.concatenate([key_heads, value_heads], axis=-1)
        fringe = with_halo(key_value, (("sp", 0),), reach_rows, False)
        attended = attend(query_heads, fringe, seg_own, seg_fringe, offset_bias[layer_index])
        attended = attended.reshape(token_count, head_count * HEAD_DIM)
        partial_sums = jnp.dot(
            attended, collected[3][layer_index], preferred_element_type=jnp.float32
        )
        stream = (
            lax.psum_scatter(
                partial_sums.astype(jnp.bfloat16), "tp", scatter_dimension=1, tiled=True
            )
            .astype(jnp.float32)
            .astype(jnp.bfloat16)
        )
    return stream


def solution(mesh):
    return jax.shard_map(
        body,
        mesh=mesh,
        in_specs=(
            P("sp", "tp"),
            P(),
            P(None, "sp", "tp"),
            P(None, "sp", "tp"),
            P(None, "sp", "tp"),
            P(None, "tp", "sp"),
            P(None, "tp", None, None),
            P("sp"),
        ),
        out_specs=P("sp", "tp"),
        check_vma=False,
    )
```

profile of v0, /device:TPU:0, one launch (start us, length us, event | category | flops | bytes accessed | tf_op | source)
XLA Modules:
  0.0 309.1 jit_solution(167499018848324964)
XLA Ops:
  9.5 4.9 %collective-permute-start.2 = (s32[4,32]{1,0:T(4,128)S(1)}, s32[4,32]{1,0:T(4,128)S(1)}, u32[]{:S(2)}, u32[]{:S(2)}) collective-permute-start(s32[4,32]{1,0:T(4,128)S(1)} %reshape.186), channel_id=1, source_target_pairs={{0,4},{4,8},{8,12},{12,16},{16,20},{20,24},{24,28},{1,5},{5,9},{9,... | collective-permute-start | bytes 1544 | tf_op jit(solution)/shard_map/ppermute | solution.py:21
  15.8 6.0 %all_gather.21 = bf16[128,1024]{1,0:T(8,128)(2,1)S(1)} all-gather(bf16[128,256]{1,0:T(8,128)(2,1)} %param.8), channel_id=1, replica_groups=mesh['sp'=8,'tp'=4] {'tp'}, dimensions={1}, use_global_device_ids=true | all-gather | bytes 327680 | tf_op jit(solution)/shard_map/all_gather | solution.py:84
  23.8 3.5 %gather_fusion = f32[1024,4,8]{2,1,0:T(4,128)S(1)} fusion(f32[4,8,16]{1,0,2:T(4,128)S(1)} %bitcast.251, s32[1024]{0:T(1024)S(1)} %broadcast_clamp_fusion), kind=kCustom, calls=%fused_computation | custom fusion | bytes 266240 | tf_op jit(solution)/shard_map/gather | solution.py:55
  29.0 27.4 %all-gather.5.cloned.1.call-done = bf16[3,1024,256]{2,1,0:T(8,128)(2,1)} async-done(((bf16[3,128,256]{2,1,0:T(8,128)(2,1)}), bf16[3,1024,256]{2,1,0:T(8,128)(2,1)}) %all-gather.5.cloned.1.call-update) | async-done | bytes 1572880 | tf_op jit(solution)/shard_map/all_gather | solution.py:78
  58.4 42.8 %all-gather.7.cloned.1.call-done = bf16[3,1024,256]{2,1,0:T(8,128)(2,1)} async-done(((bf16[3,128,256]{2,1,0:T(8,128)(2,1)}), bf16[3,1024,256]{2,1,0:T(8,128)(2,1)}) %all-gather.7.cloned.1.call-update) | async-done | bytes 1572880 | tf_op jit(solution)/shard_map/all_gather | solution.py:79
  102.8 2.5 collective-permute-start
  106.5 39.4 %all-gather.9.cloned.1.call-done = bf16[3,1024,256]{2,1,0:T(8,128)(2,1)} async-done(((bf16[3,128,256]{2,1,0:T(8,128)(2,1)}), bf16[3,1024,256]{2,1,0:T(8,128)(2,1)}) %all-gather.9.cloned.1.call-update) | async-done | bytes 1572880 | tf_op jit(solution)/shard_map/all_gather | solution.py:77
  150.8 39.8 %all-gather.11.cloned.1.call-done = bf16[3,256,1024]{2,1,0:T(8,128)(2,1)} async-done(((bf16[3,256,128]{2,1,0:T(8,128)(2,1)}), bf16[3,256,1024]{2,1,0:T(8,128)(2,1)}) %all-gather.11.cloned.1.call-update) | async-done | bytes 1572880 | tf_op jit(solution)/shard_map/all_gather | solution.py:80
  190.7 2.0 convolution_convert_fusion.2
  192.8 3.6 %gather_fusion.1 = f32[1024,4,8]{2,1,0:T(4,128)S(1)} fusion(f32[4,8,16]{1,0,2:T(4,128)S(1)} %bitcast.252, s32[1024]{0:T(1024)S(1)} %broadcast_clamp_fusion), kind=kCustom, calls=%fused_computation.1 | custom fusion | bytes 266240 | tf_op jit(solution)/shard_map/gather | solution.py:55
  197.6 13.6 %reduce-scatter.4.cloned.1.call-done = bf16[128,256]{1,0:T(8,128)(2,1)} async-done(((bf16[128,1024]{1,0:T(8,128)(2,1)}), bf16[128,256]{1,0:T(8,128)(2,1)}) %reduce-scatter.4.cloned.1.call-update) | async-done | bytes 65552 | tf_op jit(solution)/shard_map/reduce_scatter | solution.py:106
  211.2 6.0 %all_gather.26 = bf16[128,1024]{1,0:T(8,128)(2,1)S(1)} all-gather(bf16[128,256]{1,0:T(8,128)(2,1)} %reduce-scatter.4.cloned.1.call-done), channel_id=1, replica_groups=mesh['sp'=8,'tp'=4] {'tp'}, dimensions={1}, use_global_device_ids=true | all-gather | bytes 327680 | tf_op jit(solution)/shard_map/all_gather | solution.py:84
  220.9 3.4 %collective-permute-start.4 = (bf16[4,32,4,128]{3,1,2,0:T(8,128)(2,1)S(1)}, bf16[4,32,4,128]{3,1,2,0:T(8,128)(2,1)S(1)}, u32[]{:S(2)}, u32[]{:S(2)}) collective-permute-start(bf16[4,32,4,128]{3,1,2,0:T(8,128)(2,1)S(1)} %pad_maximum_fusion.4), channel_id=1, source_target_pairs={{0,4},{4,8},{8,12},{12,16},{16,20},{20,24},{24,28},{1,5},{5,9},{9,... | collective-permute-start | bytes 393224 | tf_op jit(solution)/shard_map/ppermute | solution.py:21
  224.3 1.5 collective-permute-start.5
  227.7 3.9 %collective-permute-done.5 = bf16[4,32,4,128]{3,1,2,0:T(8,128)(2,1)S(1)} collective-permute-done((bf16[4,32,4,128]{3,1,2,0:T(8,128)(2,1)S(1)}, bf16[4,32,4,128]{3,1,2,0:T(8,128)(2,1)S(1)}, u32[]{:S(2)}, u32[]{:S(2)}) %collective-permute-start.5) | collective-permute-done | bytes 131104 | tf_op jit(solution)/shard_map/ppermute | solution.py:22
  234.6 2.0 convolution_convert_fusion.1
  236.7 3.5 %gather_fusion.2 = f32[1024,4,8]{2,1,0:T(4,128)S(1)} fusion(f32[4,8,16]{1,0,2:T(4,128)S(1)} %bitcast.250, s32[1024]{0:T(1024)S(1)} %broadcast_clamp_fusion), kind=kCustom, calls=%fused_computation.2 | custom fusion | bytes 266240 | tf_op jit(solution)/shard_map/gather | solution.py:55
  241.5 15.2 %reduce-scatter.6.cloned.1.call-done = bf16[128,256]{1,0:T(8,128)(2,1)} async-done(((bf16[128,1024]{1,0:T(8,128)(2,1)}), bf16[128,256]{1,0:T(8,128)(2,1)}) %reduce-scatter.6.cloned.1.call-update) | async-done | bytes 65552 | tf_op jit(solution)/shard_map/reduce_scatter | solution.py:106
  256.7 6.0 %all_gather.27 = bf16[128,1024]{1,0:T(8,128)(2,1)S(1)} all-gather(bf16[128,256]{1,0:T(8,128)(2,1)} %reduce-scatter.6.cloned.1.call-done), channel_id=1, replica_groups=mesh['sp'=8,'tp'=4] {'tp'}, dimensions={1}, use_global_device_ids=true | all-gather | bytes 327680 | tf_op jit(solution)/shard_map/all_gather | solution.py:84
  262.9 1.3 fusion.13
  266.4 3.4 %collective-permute-start.6 = (bf16[4,32,4,128]{3,1,2,0:T(8,128)(2,1)S(1)}, bf16[4,32,4,128]{3,1,2,0:T(8,128)(2,1)S(1)}, u32[]{:S(2)}, u32[]{:S(2)}) collective-permute-start(bf16[4,32,4,128]{3,1,2,0:T(8,128)(2,1)S(1)} %pad_maximum_fusion.5), channel_id=1, source_target_pairs={{0,4},{4,8},{8,12},{12,16},{16,20},{20,24},{24,28},{1,5},{5,9},{9,... | collective-permute-start | bytes 393224 | tf_op jit(solution)/shard_map/ppermute | solution.py:21
  273.1 4.1 %collective-permute-done.7 = bf16[4,32,4,128]{3,1,2,0:T(8,128)(2,1)S(1)} collective-permute-done((bf16[4,32,4,128]{3,1,2,0:T(8,128)(2,1)S(1)}, bf16[4,32,4,128]{3,1,2,0:T(8,128)(2,1)S(1)}, u32[]{:S(2)}, u32[]{:S(2)}) %collective-permute-start.7) | collective-permute-done | bytes 131104 | tf_op jit(solution)/shard_map/ppermute | solution.py:22
  280.1 2.0 convolution_convert_fusion
  282.1 20.2 %reduce-scatter.8.cloned.1.call-done = bf16[128,256]{1,0:T(8,128)(2,1)} async-done(((bf16[128,1024]{1,0:T(8,128)(2,1)}), bf16[128,256]{1,0:T(8,128)(2,1)}) %reduce-scatter.8.cloned.1.call-update) | async-done | bytes 65552 | tf_op jit(solution)/shard_map/reduce_scatter | solution.py:106
  (141 shorter events, 37.0 us)
Async XLA Ops:
  6.5 49.9 %all-gather.5.cloned.1.call-start = ((), (), s32[]{:S(2)}) async-start(), calls=%async_computation.3 | async-start | bytes 1769472 | tf_op jit(solution)/shard_map/all_gather | solution.py:78
  7.3 93.9 %all-gather.7.cloned.1.call-start = ((), (), s32[]{:S(2)}) async-start(), calls=%async_computation.4 | async-start | bytes 1769472 | tf_op jit(solution)/shard_map/all_gather | solution.py:79
  8.0 137.9 %all-gather.9.cloned.1.call-start = ((), (), s32[]{:S(2)}) async-start(), calls=%async_computation.5 | async-start | bytes 1769472 | tf_op jit(solution)/shard_map/all_gather | solution.py:77
  8.7 181.9 %all-gather.11.cloned.1.call-start = ((), (), s32[]{:S(2)}) async-start(), calls=%async_computation.6 | async-start | bytes 1769472 | tf_op jit(solution)/shard_map/all_gather | solution.py:80
  9.5 19.1 %collective-permute-start.2 = (s32[4,32]{1,0:T(4,128)S(1)}, s32[4,32]{1,0:T(4,128)S(1)}, u32[]{:S(2)}, u32[]{:S(2)}) collective-permute-start(s32[4,32]{1,0:T(4,128)S(1)} %reshape.186), channel_id=1, source_target_pairs={{0,4},{4,8},{8,12},{12,16},{16,20},{20,24},{24,28},{1,5},{5,9},{9,... | collective-permute-start | bytes 1544 | tf_op jit(solution)/shard_map/ppermute | solution.py:21
  14.4 14.2 %collective-permute-start.3 = (s32[4,32]{1,0:T(4,128)S(1)}, s32[4,32]{1,0:T(4,128)S(1)}, u32[]{:S(2)}, u32[]{:S(2)}) collective-permute-start(s32[4,32]{1,0:T(4,128)S(1)} %reshape.186), channel_id=1, source_target_pairs={{4,0},{8,4},{12,8},{16,12},{20,16},{24,20},{28,24},{5,1},{9,5},{13... | collective-permute-start | bytes 1544 | tf_op jit(solution)/shard_map/ppermute | solution.py:22
  15.7 195.5 %reduce-scatter.4.cloned.1.call-start = ((), (), s32[]{:S(2)}) async-start(), calls=%async_computation.7 | async-start | bytes 327680 | tf_op jit(solution)/shard_map/reduce_scatter | solution.py:106
  102.8 45.1 %collective-permute-start = (bf16[4,32,4,128]{3,1,2,0:T(8,128)(2,1)S(1)}, bf16[4,32,4,128]{3,1,2,0:T(8,128)(2,1)S(1)}, u32[]{:S(2)}, u32[]{:S(2)}) collective-permute-start(bf16[4,32,4,128]{3,1,2,0:T(8,128)(2,1)S(1)} %pad_maximum_fusion.3), channel_id=1, source_target_pairs={{0,4},{4,8},{8,12},{12,16},{16,20},{20,24},{24,28},{1,5},{5,9},{9,... | collective-permute-start | bytes 393224 | tf_op jit(solution)/shard_map/ppermute | solution.py:21
  105.2 42.7 %collective-permute-start.1 = (bf16[4,32,4,128]{3,1,2,0:T(8,128)(2,1)S(1)}, bf16[4,32,4,128]{3,1,2,0:T(8,128)(2,1)S(1)}, u32[]{:S(2)}, u32[]{:S(2)}) collective-permute-start(bf16[4,32,4,128]{3,1,2,0:T(8,128)(2,1)S(1)} %pad_maximum_fusion.3), channel_id=1, source_target_pairs={{4,0},{8,4},{12,8},{16,12},{20,16},{24,20},{28,24},{5,1},{9,5},{13... | collective-permute-start | bytes 393224 | tf_op jit(solution)/shard_map/ppermute | solution.py:22
  192.7 64.1 %reduce-scatter.6.cloned.1.call-start = ((), (), s32[]{:S(2)}) async-start(), calls=%async_computation.8 | async-start | bytes 327680 | tf_op jit(solution)/shard_map/reduce_scatter | solution.py:106
  220.9 6.8 %collective-permute-start.4 = (bf16[4,32,4,128]{3,1,2,0:T(8,128)(2,1)S(1)}, bf16[4,32,4,128]{3,1,2,0:T(8,128)(2,1)S(1)}, u32[]{:S(2)}, u32[]{:S(2)}) collective-permute-start(bf16[4,32,4,128]{3,1,2,0:T(8,128)(2,1)S(1)} %pad_maximum_fusion.4), channel_id=1, source_target_pairs={{0,4},{4,8},{8,12},{12,16},{16,20},{20,24},{24,28},{1,5},{5,9},{9,... | collective-permute-start | bytes 393224 | tf_op jit(solution)/shard_map/ppermute | solution.py:21
  224.3 7.4 %collective-permute-start.5 = (bf16[4,32,4,128]{3,1,2,0:T(8,128)(2,1)S(1)}, bf16[4,32,4,128]{3,1,2,0:T(8,128)(2,1)S(1)}, u32[]{:S(2)}, u32[]{:S(2)}) collective-permute-start(bf16[4,32,4,128]{3,1,2,0:T(8,128)(2,1)S(1)} %pad_maximum_fusion.4), channel_id=1, source_target_pairs={{4,0},{8,4},{12,8},{16,12},{20,16},{24,20},{28,24},{5,1},{9,5},{13... | collective-permute-start | bytes 393224 | tf_op jit(solution)/shard_map/ppermute | solution.py:22
  236.6 65.7 %reduce-scatter.8.cloned.1.call-start = ((), (), s32[]{:S(2)}) async-start(), calls=%async_computation.9 | async-start | bytes 327680 | tf_op jit(solution)/shard_map/reduce_scatter | solution.py:106
  266.4 6.6 %collective-permute-start.6 = (bf16[4,32,4,128]{3,1,2,0:T(8,128)(2,1)S(1)}, bf16[4,32,4,128]{3,1,2,0:T(8,128)(2,1)S(1)}, u32[]{:S(2)}, u32[]{:S(2)}) collective-permute-start(bf16[4,32,4,128]{3,1,2,0:T(8,128)(2,1)S(1)} %pad_maximum_fusion.5), channel_id=1, source_target_pairs={{0,4},{4,8},{8,12},{12,16},{16,20},{20,24},{24,28},{1,5},{5,9},{9,... | collective-permute-start | bytes 393224 | tf_op jit(solution)/shard_map/ppermute | solution.py:21
  269.8 7.4 %collective-permute-start.7 = (bf16[4,32,4,128]{3,1,2,0:T(8,128)(2,1)S(1)}, bf16[4,32,4,128]{3,1,2,0:T(8,128)(2,1)S(1)}, u32[]{:S(2)}, u32[]{:S(2)}) collective-permute-start(bf16[4,32,4,128]{3,1,2,0:T(8,128)(2,1)S(1)} %pad_maximum_fusion.5), channel_id=1, source_target_pairs={{4,0},{8,4},{12,8},{16,12},{20,16},{24,20},{28,24},{5,1},{9,5},{13... | collective-permute-start | bytes 393224 | tf_op jit(solution)/shard_map/ppermute | solution.py:22
Sparse Core Ops, SparseCore 0:
  9.5 46.8 all-gather.4
  58.6 42.5 all-gather.6
  103.4 42.5 all-gather.8
  147.8 42.7 all-gather.10
  193.0 18.2 reduce-scatter.3
  236.7 19.9 reduce-scatter.5
  282.2 20.0 reduce-scatter.7
where the time goes:
time: 310 us; the launch traced here: 309 us
  waiting for transfers between devices  209 us (67%)
  matrix products  23 us (7%)
  starting transfers between devices  19.7 us (6%)
  local copies, waits for them, and re-layouts  19.3 us (6%)
  blocking collectives  17.9 us (6%)
  between operations  14.2 us (5%)
  other arithmetic  6.3 us (2%)
    reduce_scatter x3, waiting for transfers between devices, body(): lax.psum_scatter(partial_sums.astype(jnp.bfloat16), 'tp', scatter_dimensi...  49 us
    all_gather x1, waiting for transfers between devices, body(): lax.all_gather(w_value, 'sp', axis=1, tiled=True)  42.8 us
    all_gather x1, waiting for transfers between devices, body(): lax.all_gather(w_out, 'sp', axis=2, tiled=True)  39.8 us
    all_gather x1, waiting for transfers between devices, body(): lax.all_gather(w_query, 'sp', axis=1, tiled=True)  39.4 us
    all_gather x1, waiting for transfers between devices, body(): lax.all_gather(w_key, 'sp', axis=1, tiled=True)  27.4 us
    all_gather x3, blocking collectives, body(): gathered = lax.all_gather(stream, 'tp', axis=1, tiled=True)  17.9 us
    gather x6, local copies, waits for them, and re-layouts, attend(): bias_table = bias_layer[:, :, jnp.clip(col_offset, 0, WIN_COLS - 1)]  14.4 us
    ppermute x4, starting transfers between devices, with_halo(): before = lax.ppermute(last, axis, up)  14.1 us
  transfers between devices with their start and end apart: 15, of which 9 were waited for; matrix products, arithmetic and copies ran while one was open for 10% of the time, Pallas kernels for 0%

commit v1 on v0

--- a/solution.py
+++ b/solution.py
@@ -9,6 +9,34 @@
 LAYERS = 3
 GRID_W = 32
 EPS = 1e-06
+
+
+def bind_the_shapes(on_dim, xx):
+    axis_name = "sp"
+    f_now = lax.axis_size(axis_name)
+    far_arr = lax.axis_index(axis_name)
+    seen_now, arr_now, wide_out = (f_now, far_arr, xx.shape[on_dim])
+    pages = [h * seen_now if k == on_dim else h for k, h in enumerate(xx.shape)]
+    fresh = jnp.zeros(pages, xx.dtype)
+    latest = outcome_arr = xx
+    reply = lax.dynamic_update_slice_in_dim(fresh, xx, arr_now * wide_out, axis=on_dim)
+    for k0 in range(1, seen_now // 2 + 1):
+        latest = lax.ppermute(
+            latest, axis_name=axis_name, perm=[(k, (k + 1) % seen_now) for k in range(seen_now)]
+        )
+        reply = lax.dynamic_update_slice_in_dim(
+            reply, latest, (arr_now - k0) % seen_now * wide_out, axis=on_dim
+        )
+        if 2 * k0 < seen_now:
+            outcome_arr = lax.ppermute(
+                outcome_arr,
+                axis_name=axis_name,
+                perm=[(k, (k - 1) % seen_now) for k in range(seen_now)],
+            )
+            reply = lax.dynamic_update_slice_in_dim(
+                reply, outcome_arr, (arr_now + k0) % seen_now * wide_out, axis=on_dim
+            )
+    return reply
 
 
 def with_halo(shard, sides, width, wrap):
@@ -77,7 +105,7 @@
         lax.all_gather(w_query, "sp", axis=1, tiled=True),
         lax.all_gather(w_key, "sp", axis=1, tiled=True),
         lax.all_gather(w_value, "sp", axis=1, tiled=True),
-        lax.all_gather(w_out, "sp", axis=2, tiled=True),
+        bind_the_shapes(2, xx=w_out),
     )
     stream = tokens
     for layer_index in range(LAYERS):

time: 310 us -> 279 us (0.900)
  waiting for transfers between devices: 209 us -> 150 us
  local copies, waits for them, and re-layouts: 19.3 us -> 37.1 us
  starting transfers between devices: 19.7 us -> 32.2 us
  matrix products: 23 us -> 19.9 us
    all_gather x1 -> x0, waiting for transfers between devices: 39.8 us -> none  [body(): lax.all_gather(w_out, 'sp', axis=2, tiled=True)]
    ppermute x0 -> x7, waiting for transfers between devices: none -> 28.7 us  [the longest x4 28.2 us: bind_the_shapes(): lax.ppermute(latest, axis_name=axis_name, perm=[(k, (k + 1) % seen_now) f...]
    all_gather x1, waiting for transfers between devices: 27.4 us -> 0.02 us  [body(): lax.all_gather(w_key, 'sp', axis=1, tiled=True)]
    gather x6, local copies, waits for them, and re-layouts: 14.4 us -> 30.9 us  [attend(): bias_table = bias_layer[:, :, jnp.clip(col_offset, 0, WIN_COLS - 1)]]
    ppermute x0 -> x7, starting transfers between devices: none -> 16.2 us  [the longest x4 8.2 us: bind_the_shapes(): lax.ppermute(latest, axis_name=axis_name, perm=[(k, (k + 1) % seen_now) f...]
    reduce_scatter x3, waiting for transfers between devices: 49 us -> 38.1 us  [body(): lax.psum_scatter(partial_sums.astype(jnp.bfloat16), 'tp', scatter_dimensi...]
    all_gather x1, waiting for transfers between devices: 42.8 us -> 34.5 us  [body(): lax.all_gather(w_value, 'sp', axis=1, tiled=True)]
    ppermute x4, starting transfers between devices: 14.1 us -> 10.5 us  [with_halo(): before = lax.ppermute(last, axis, up)]
  transfers between devices with their start and end apart: 15 -> 21, of which waited for: 9 -> 11; matrix products, arithmetic and copies ran while one was open for 10% -> 16% of each run, Pallas kernels for 0% -> 0%
where the time goes in v1:
time: 279 us; the launch traced here: 278 us
  waiting for transfers between devices  150 us (54%)
  local copies, waits for them, and re-layouts  37.1 us (13%)
  starting transfers between devices  32.2 us (12%)
  matrix products  19.9 us (7%)
  blocking collectives  18.1 us (6%)
  between operations  14.5 us (5%)
  other arithmetic  6.3 us (2%)
    all_gather x1, waiting for transfers between devices, body(): lax.all_gather(w_query, 'sp', axis=1, tiled=True)  39.1 us
    reduce_scatter x3, waiting for transfers between devices, body(): lax.psum_scatter(partial_sums.astype(jnp.bfloat16), 'tp', scatter_dimensi...  38.1 us
    all_gather x1, waiting for transfers between devices, body(): lax.all_gather(w_value, 'sp', axis=1, tiled=True)  34.5 us
    gather x6, local copies, waits for them, and re-layouts, attend(): bias_table = bias_layer[:, :, jnp.clip(col_offset, 0, WIN_COLS - 1)]  30.9 us
    ppermute x4, waiting for transfers between devices, bind_the_shapes(): lax.ppermute(latest, axis_name=axis_name, perm=[(k, (k + 1) % seen_now) f...  28.2 us
    all_gather x3, blocking collectives, body(): gathered = lax.all_gather(stream, 'tp', axis=1, tiled=True)  18.1 us
    ppermute x4, starting transfers between devices, with_halo(): before = lax.ppermute(last, axis, up)  10.5 us
    ppermute x4, starting transfers between devices, bind_the_shapes(): lax.ppermute(latest, axis_name=axis_name, perm=[(k, (k + 1) % seen_now) f...  8.2 us
  transfers between devices with their start and end apart: 21, of which 11 were waited for; matrix products, arithmetic and copies ran while one was open for 16% of the time, Pallas kernels for 0%

profile of v1, /device:TPU:0, one launch (start us, length us, event | category | flops | bytes accessed | tf_op | source)
XLA Modules:
  0.0 278.0 jit_solution(7077425457252639507)
XLA Ops:
  8.1 3.0 %collective-permute-start.4 = (bf16[3,256,128]{2,1,0:T(8,128)(2,1)}, bf16[3,256,128]{2,1,0:T(8,128)(2,1)S(1)}, u32[]{:S(2)}, u32[]{:S(2)}) collective-permute-start(bf16[3,256,128]{2,1,0:T(8,128)(2,1)} %param.13), channel_id=1, source_target_pairs={{0,4},{4,8},{8,12},{12,16},{16,20},{20,24},{24,28},{28,0},{1,5},{5... | collective-permute-start | bytes 589832 | tf_op jit(solution)/shard_map/ppermute | solution.py:24
  11.1 3.1 %collective-permute-start.5 = (bf16[3,256,128]{2,1,0:T(8,128)(2,1)}, bf16[3,256,128]{2,1,0:T(8,128)(2,1)S(1)}, u32[]{:S(2)}, u32[]{:S(2)}) collective-permute-start(bf16[3,256,128]{2,1,0:T(8,128)(2,1)} %param.13), channel_id=1, source_target_pairs={{0,28},{4,0},{8,4},{12,8},{16,12},{20,16},{24,20},{28,24},{1,29},{... | collective-permute-start | bytes 589832 | tf_op jit(solution)/shard_map/ppermute | solution.py:31
  17.8 6.1 %all_gather.18 = bf16[128,1024]{1,0:T(8,128)(2,1)S(1)} all-gather(bf16[128,256]{1,0:T(8,128)(2,1)} %param.8), channel_id=1, replica_groups=mesh['sp'=8,'tp'=4] {'tp'}, dimensions={1}, use_global_device_ids=true | all-gather | bytes 327680 | tf_op jit(solution)/shard_map/all_gather | solution.py:112
  26.7 7.9 %gather_fusion = f32[1024,4,8]{2,1,0:T(4,128)} fusion(f32[4,8,16]{1,0,2:T(4,128)S(1)} %bitcast.250, s32[1024]{0:T(1024)S(1)} %broadcast_clamp_fusion), kind=kCustom, calls=%fused_computation | custom fusion | bytes 266240 | tf_op jit(solution)/shard_map/gather | solution.py:83
  37.5 2.7 collective-permute-start.6
  40.2 2.5 collective-permute-start.7
  42.8 10.9 %collective-permute-done.6 = bf16[3,256,128]{2,1,0:T(8,128)(2,1)S(1)} collective-permute-done((bf16[3,256,128]{2,1,0:T(8,128)(2,1)S(1)}, bf16[3,256,128]{2,1,0:T(8,128)(2,1)S(1)}, u32[]{:S(2)}, u32[]{:S(2)}) %collective-permute-start.6) | collective-permute-done | bytes 196640 | tf_op jit(solution)/shard_map/ppermute | solution.py:24
  53.7 2.5 collective-permute-start.8
  59.2 8.8 %collective-permute-done.8 = bf16[3,256,128]{2,1,0:T(8,128)(2,1)S(1)} collective-permute-done((bf16[3,256,128]{2,1,0:T(8,128)(2,1)S(1)}, bf16[3,256,128]{2,1,0:T(8,128)(2,1)S(1)}, u32[]{:S(2)}, u32[]{:S(2)}) %collective-permute-start.8) | collective-permute-done | bytes 196640 | tf_op jit(solution)/shard_map/ppermute | solution.py:24
  68.2 8.5 %collective-permute-done.10 = bf16[3,256,128]{2,1,0:T(8,128)(2,1)S(1)} collective-permute-done((bf16[3,256,128]{2,1,0:T(8,128)(2,1)S(1)}, bf16[3,256,128]{2,1,0:T(8,128)(2,1)S(1)}, u32[]{:S(2)}, u32[]{:S(2)}) %collective-permute-start.10) | collective-permute-done | bytes 196640 | tf_op jit(solution)/shard_map/ppermute | solution.py:24
  78.6 34.5 %all-gather.6.cloned.1.call-done = bf16[3,1024,256]{2,1,0:T(8,128)(2,1)} async-done(((bf16[3,128,256]{2,1,0:T(8,128)(2,1)}), bf16[3,1024,256]{2,1,0:T(8,128)(2,1)}) %all-gather.6.cloned.1.call-update) | async-done | bytes 1572880 | tf_op jit(solution)/shard_map/all_gather | solution.py:107
  114.8 2.5 collective-permute-start
  118.6 39.1 %all-gather.8.cloned.1.call-done = bf16[3,1024,256]{2,1,0:T(8,128)(2,1)} async-done(((bf16[3,128,256]{2,1,0:T(8,128)(2,1)}), bf16[3,1024,256]{2,1,0:T(8,128)(2,1)}) %all-gather.8.cloned.1.call-update) | async-done | bytes 1572880 | tf_op jit(solution)/shard_map/all_gather | solution.py:105
  163.7 7.9 %gather_fusion.1 = f32[1024,4,8]{2,1,0:T(4,128)} fusion(f32[4,8,16]{1,0,2:T(4,128)S(1)} %bitcast.252, s32[1024]{0:T(1024)S(1)} %broadcast_clamp_fusion), kind=kCustom, calls=%fused_computation.1 | custom fusion | bytes 266240 | tf_op jit(solution)/shard_map/gather | solution.py:83
  174.0 8.1 %reduce-scatter.4.cloned.1.call-done = bf16[128,256]{1,0:T(8,128)(2,1)} async-done(((bf16[128,1024]{1,0:T(8,128)(2,1)}), bf16[128,256]{1,0:T(8,128)(2,1)}) %reduce-scatter.4.cloned.1.call-update) | async-done | bytes 65552 | tf_op jit(solution)/shard_map/reduce_scatter | solution.py:134
  182.1 6.0 %all_gather.22 = bf16[128,1024]{1,0:T(8,128)(2,1)S(1)} all-gather(bf16[128,256]{1,0:T(8,128)(2,1)} %reduce-scatter.4.cloned.1.call-done), channel_id=1, replica_groups=mesh['sp'=8,'tp'=4] {'tp'}, dimensions={1}, use_global_device_ids=true | all-gather | bytes 327680 | tf_op jit(solution)/shard_map/all_gather | solution.py:112
  191.8 3.4 %collective-permute-start.11 = (bf16[4,32,4,128]{3,1,2,0:T(8,128)(2,1)S(1)}, bf16[4,32,4,128]{3,1,2,0:T(8,128)(2,1)S(1)}, u32[]{:S(2)}, u32[]{:S(2)}) collective-permute-start(bf16[4,32,4,128]{3,1,2,0:T(8,128)(2,1)S(1)} %pad_maximum_fusion.4), channel_id=1, source_target_pairs={{0,4},{4,8},{8,12},{12,16},{16,20},{20,24},{24,28},{1,5},{5,9},{9,... | collective-permute-start | bytes 393224 | tf_op jit(solution)/shard_map/ppermute | solution.py:49
  198.6 3.9 %collective-permute-done.12 = bf16[4,32,4,128]{3,1,2,0:T(8,128)(2,1)S(1)} collective-permute-done((bf16[4,32,4,128]{3,1,2,0:T(8,128)(2,1)S(1)}, bf16[4,32,4,128]{3,1,2,0:T(8,128)(2,1)S(1)}, u32[]{:S(2)}, u32[]{:S(2)}) %collective-permute-start.12) | collective-permute-done | bytes 131104 | tf_op jit(solution)/shard_map/ppermute | solution.py:50
  206.6 7.9 %gather_fusion.2 = f32[1024,4,8]{2,1,0:T(4,128)} fusion(f32[4,8,16]{1,0,2:T(4,128)S(1)} %bitcast.251, s32[1024]{0:T(1024)S(1)} %broadcast_clamp_fusion), kind=kCustom, calls=%fused_computation.2 | custom fusion | bytes 266240 | tf_op jit(solution)/shard_map/gather | solution.py:83
  216.9 9.7 %reduce-scatter.6.cloned.1.call-done = bf16[128,256]{1,0:T(8,128)(2,1)} async-done(((bf16[128,1024]{1,0:T(8,128)(2,1)}), bf16[128,256]{1,0:T(8,128)(2,1)}) %reduce-scatter.6.cloned.1.call-update) | async-done | bytes 65552 | tf_op jit(solution)/shard_map/reduce_scatter | solution.py:134
  226.6 6.0 %all_gather.23 = bf16[128,1024]{1,0:T(8,128)(2,1)S(1)} all-gather(bf16[128,256]{1,0:T(8,128)(2,1)} %reduce-scatter.6.cloned.1.call-done), channel_id=1, replica_groups=mesh['sp'=8,'tp'=4] {'tp'}, dimensions={1}, use_global_device_ids=true | all-gather | bytes 327680 | tf_op jit(solution)/shard_map/all_gather | solution.py:112
  236.3 3.4 %collective-permute-start.13 = (bf16[4,32,4,128]{3,1,2,0:T(8,128)(2,1)S(1)}, bf16[4,32,4,128]{3,1,2,0:T(8,128)(2,1)S(1)}, u32[]{:S(2)}, u32[]{:S(2)}) collective-permute-start(bf16[4,32,4,128]{3,1,2,0:T(8,128)(2,1)S(1)} %pad_maximum_fusion.5), channel_id=1, source_target_pairs={{0,4},{4,8},{8,12},{12,16},{16,20},{20,24},{24,28},{1,5},{5,9},{9,... | collective-permute-start | bytes 393224 | tf_op jit(solution)/shard_map/ppermute | solution.py:49
  243.0 4.1 %collective-permute-done.14 = bf16[4,32,4,128]{3,1,2,0:T(8,128)(2,1)S(1)} collective-permute-done((bf16[4,32,4,128]{3,1,2,0:T(8,128)(2,1)S(1)}, bf16[4,32,4,128]{3,1,2,0:T(8,128)(2,1)S(1)}, u32[]{:S(2)}, u32[]{:S(2)}) %collective-permute-start.14) | collective-permute-done | bytes 131104 | tf_op jit(solution)/shard_map/ppermute | solution.py:50
  250.9 20.2 %reduce-scatter.8.cloned.1.call-done = bf16[128,256]{1,0:T(8,128)(2,1)} async-done(((bf16[128,1024]{1,0:T(8,128)(2,1)}), bf16[128,256]{1,0:T(8,128)(2,1)}) %reduce-scatter.8.cloned.1.call-update) | async-done | bytes 65552 | tf_op jit(solution)/shard_map/reduce_scatter | solution.py:134
  (165 shorter events, 50.7 us)
Async XLA Ops:
  6.5 20.1 %copy-start = (bf16[3,256,128]{2,1,0:T(8,128)(2,1)S(1)}, bf16[3,256,128]{2,1,0:T(8,128)(2,1)}, u32[]{:S(2)}) copy-start(bf16[3,256,128]{2,1,0:T(8,128)(2,1)} %param.13) | copy-start | bytes 589828
  6.5 70.2 %all-gather.4.cloned.1.call-start = ((), (), s32[]{:S(2)}) async-start(), calls=%async_computation.3 | async-start | bytes 1769472 | tf_op jit(solution)/shard_map/all_gather | solution.py:106
  7.3 105.8 %all-gather.6.cloned.1.call-start = ((), (), s32[]{:S(2)}) async-start(), calls=%async_computation.4 | async-start | bytes 1769472 | tf_op jit(solution)/shard_map/all_gather | solution.py:107
  8.0 149.7 %all-gather.8.cloned.1.call-start = ((), (), s32[]{:S(2)}) async-start(), calls=%async_computation.5 | async-start | bytes 1769472 | tf_op jit(solution)/shard_map/all_gather | solution.py:105
  8.1 29.4 %collective-permute-start.4 = (bf16[3,256,128]{2,1,0:T(8,128)(2,1)}, bf16[3,256,128]{2,1,0:T(8,128)(2,1)S(1)}, u32[]{:S(2)}, u32[]{:S(2)}) collective-permute-start(bf16[3,256,128]{2,1,0:T(8,128)(2,1)} %param.13), channel_id=1, source_target_pairs={{0,4},{4,8},{8,12},{12,16},{16,20},{20,24},{24,28},{28,0},{1,5},{5... | collective-permute-start | bytes 589832 | tf_op jit(solution)/shard_map/ppermute | solution.py:24
  11.1 29.1 %collective-permute-start.5 = (bf16[3,256,128]{2,1,0:T(8,128)(2,1)}, bf16[3,256,128]{2,1,0:T(8,128)(2,1)S(1)}, u32[]{:S(2)}, u32[]{:S(2)}) collective-permute-start(bf16[3,256,128]{2,1,0:T(8,128)(2,1)} %param.13), channel_id=1, source_target_pairs={{0,28},{4,0},{8,4},{12,8},{16,12},{20,16},{24,20},{28,24},{1,29},{... | collective-permute-start | bytes 589832 | tf_op jit(solution)/shard_map/ppermute | solution.py:31
  14.9 22.2 %collective-permute-start.2 = (s32[4,32]{1,0:T(4,128)S(1)}, s32[4,32]{1,0:T(4,128)S(1)}, u32[]{:S(2)}, u32[]{:S(2)}) collective-permute-start(s32[4,32]{1,0:T(4,128)S(1)} %reshape.186), channel_id=1, source_target_pairs={{0,4},{4,8},{8,12},{12,16},{16,20},{20,24},{24,28},{1,5},{5,9},{9,... | collective-permute-start | bytes 1544 | tf_op jit(solution)/shard_map/ppermute | solution.py:49
  16.2 20.9 %collective-permute-start.3 = (s32[4,32]{1,0:T(4,128)S(1)}, s32[4,32]{1,0:T(4,128)S(1)}, u32[]{:S(2)}, u32[]{:S(2)}) collective-permute-start(s32[4,32]{1,0:T(4,128)S(1)} %reshape.186), channel_id=1, source_target_pairs={{4,0},{8,4},{12,8},{16,12},{20,16},{24,20},{28,24},{5,1},{9,5},{13... | collective-permute-start | bytes 1544 | tf_op jit(solution)/shard_map/ppermute | solution.py:50
  17.5 164.6 %reduce-scatter.4.cloned.1.call-start = ((), (), s32[]{:S(2)}) async-start(), calls=%async_computation.6 | async-start | bytes 327680 | tf_op jit(solution)/shard_map/reduce_scatter | solution.py:134
  37.5 16.2 %collective-permute-start.6 = (bf16[3,256,128]{2,1,0:T(8,128)(2,1)S(1)}, bf16[3,256,128]{2,1,0:T(8,128)(2,1)S(1)}, u32[]{:S(2)}, u32[]{:S(2)}) collective-permute-start(bf16[3,256,128]{2,1,0:T(8,128)(2,1)S(1)} %collective-permute-done.4), channel_id=1, source_target_pairs={{0,4},{4,8},{8,12},{12,16},{16,20},{20,24},{24,28},{28,0},{1,5},{5... | collective-permute-start | bytes 589832 | tf_op jit(solution)/shard_map/ppermute | solution.py:24
  40.2 16.5 %collective-permute-start.7 = (bf16[3,256,128]{2,1,0:T(8,128)(2,1)S(1)}, bf16[3,256,128]{2,1,0:T(8,128)(2,1)S(1)}, u32[]{:S(2)}, u32[]{:S(2)}) collective-permute-start(bf16[3,256,128]{2,1,0:T(8,128)(2,1)S(1)} %collective-permute-done.5), channel_id=1, source_target_pairs={{0,28},{4,0},{8,4},{12,8},{16,12},{20,16},{24,20},{28,24},{1,29},{... | collective-permute-start | bytes 589832 | tf_op jit(solution)/shard_map/ppermute | solution.py:31
  53.7 14.3 %collective-permute-start.8 = (bf16[3,256,128]{2,1,0:T(8,128)(2,1)S(1)}, bf16[3,256,128]{2,1,0:T(8,128)(2,1)S(1)}, u32[]{:S(2)}, u32[]{:S(2)}) collective-permute-start(bf16[3,256,128]{2,1,0:T(8,128)(2,1)S(1)} %collective-permute-done.6), channel_id=1, source_target_pairs={{0,4},{4,8},{8,12},{12,16},{16,20},{20,24},{24,28},{28,0},{1,5},{5... | collective-permute-start | bytes 589832 | tf_op jit(solution)/shard_map/ppermute | solution.py:24
  56.7 11.4 %collective-permute-start.9 = (bf16[3,256,128]{2,1,0:T(8,128)(2,1)S(1)}, bf16[3,256,128]{2,1,0:T(8,128)(2,1)S(1)}, u32[]{:S(2)}, u32[]{:S(2)}) collective-permute-start(bf16[3,256,128]{2,1,0:T(8,128)(2,1)S(1)} %collective-permute-done.7), channel_id=1, source_target_pairs={{0,28},{4,0},{8,4},{12,8},{16,12},{20,16},{24,20},{28,24},{1,29},{... | collective-permute-start | bytes 589832 | tf_op jit(solution)/shard_map/ppermute | solution.py:31
  68.0 8.7 %collective-permute-start.10 = (bf16[3,256,128]{2,1,0:T(8,128)(2,1)S(1)}, bf16[3,256,128]{2,1,0:T(8,128)(2,1)S(1)}, u32[]{:S(2)}, u32[]{:S(2)}) collective-permute-start(bf16[3,256,128]{2,1,0:T(8,128)(2,1)S(1)} %collective-permute-done.8), channel_id=1, source_target_pairs={{0,4},{4,8},{8,12},{12,16},{16,20},{20,24},{24,28},{28,0},{1,5},{5... | collective-permute-start | bytes 589832 | tf_op jit(solution)/shard_map/ppermute | solution.py:24
  114.8 44.8 %collective-permute-start = (bf16[4,32,4,128]{3,1,2,0:T(8,128)(2,1)S(1)}, bf16[4,32,4,128]{3,1,2,0:T(8,128)(2,1)S(1)}, u32[]{:S(2)}, u32[]{:S(2)}) collective-permute-start(bf16[4,32,4,128]{3,1,2,0:T(8,128)(2,1)S(1)} %pad_maximum_fusion.3), channel_id=1, source_target_pairs={{0,4},{4,8},{8,12},{12,16},{16,20},{20,24},{24,28},{1,5},{5,9},{9,... | collective-permute-start | bytes 393224 | tf_op jit(solution)/shard_map/ppermute | solution.py:49
  117.3 42.4 %collective-permute-start.1 = (bf16[4,32,4,128]{3,1,2,0:T(8,128)(2,1)S(1)}, bf16[4,32,4,128]{3,1,2,0:T(8,128)(2,1)S(1)}, u32[]{:S(2)}, u32[]{:S(2)}) collective-permute-start(bf16[4,32,4,128]{3,1,2,0:T(8,128)(2,1)S(1)} %pad_maximum_fusion.3), channel_id=1, source_target_pairs={{4,0},{8,4},{12,8},{16,12},{20,16},{24,20},{28,24},{5,1},{9,5},{13... | collective-permute-start | bytes 393224 | tf_op jit(solution)/shard_map/ppermute | solution.py:50
  163.6 63.1 %reduce-scatter.6.cloned.1.call-start = ((), (), s32[]{:S(2)}) async-start(), calls=%async_computation.7 | async-start | bytes 327680 | tf_op jit(solution)/shard_map/reduce_scatter | solution.py:134
  191.8 6.8 %collective-permute-start.11 = (bf16[4,32,4,128]{3,1,2,0:T(8,128)(2,1)S(1)}, bf16[4,32,4,128]{3,1,2,0:T(8,128)(2,1)S(1)}, u32[]{:S(2)}, u32[]{:S(2)}) collective-permute-start(bf16[4,32,4,128]{3,1,2,0:T(8,128)(2,1)S(1)} %pad_maximum_fusion.4), channel_id=1, source_target_pairs={{0,4},{4,8},{8,12},{12,16},{16,20},{20,24},{24,28},{1,5},{5,9},{9,... | collective-permute-start | bytes 393224 | tf_op jit(solution)/shard_map/ppermute | solution.py:49
  195.2 7.4 %collective-permute-start.12 = (bf16[4,32,4,128]{3,1,2,0:T(8,128)(2,1)S(1)}, bf16[4,32,4,128]{3,1,2,0:T(8,128)(2,1)S(1)}, u32[]{:S(2)}, u32[]{:S(2)}) collective-permute-start(bf16[4,32,4,128]{3,1,2,0:T(8,128)(2,1)S(1)} %pad_maximum_fusion.4), channel_id=1, source_target_pairs={{4,0},{8,4},{12,8},{16,12},{20,16},{24,20},{28,24},{5,1},{9,5},{13... | collective-permute-start | bytes 393224 | tf_op jit(solution)/shard_map/ppermute | solution.py:50
  204.2 2.3 copy-start.1
  206.5 64.7 %reduce-scatter.8.cloned.1.call-start = ((), (), s32[]{:S(2)}) async-start(), calls=%async_computation.8 | async-start | bytes 327680 | tf_op jit(solution)/shard_map/reduce_scatter | solution.py:134
  236.3 6.6 %collective-permute-start.13 = (bf16[4,32,4,128]{3,1,2,0:T(8,128)(2,1)S(1)}, bf16[4,32,4,128]{3,1,2,0:T(8,128)(2,1)S(1)}, u32[]{:S(2)}, u32[]{:S(2)}) collective-permute-start(bf16[4,32,4,128]{3,1,2,0:T(8,128)(2,1)S(1)} %pad_maximum_fusion.5), channel_id=1, source_target_pairs={{0,4},{4,8},{8,12},{12,16},{16,20},{20,24},{24,28},{1,5},{5,9},{9,... | collective-permute-start | bytes 393224 | tf_op jit(solution)/shard_map/ppermute | solution.py:49
  239.7 7.4 %collective-permute-start.14 = (bf16[4,32,4,128]{3,1,2,0:T(8,128)(2,1)S(1)}, bf16[4,32,4,128]{3,1,2,0:T(8,128)(2,1)S(1)}, u32[]{:S(2)}, u32[]{:S(2)}) collective-permute-start(bf16[4,32,4,128]{3,1,2,0:T(8,128)(2,1)S(1)} %pad_maximum_fusion.5), channel_id=1, source_target_pairs={{4,0},{8,4},{12,8},{16,12},{20,16},{24,20},{28,24},{5,1},{9,5},{13... | collective-permute-start | bytes 393224 | tf_op jit(solution)/shard_map/ppermute | solution.py:50
Sparse Core Ops, SparseCore 0:
  9.5 57.4 all-gather.3
  69.2 43.8 all-gather.5
  115.3 42.3 all-gather.7
  163.7 18.4 reduce-scatter.3
  206.6 20.0 reduce-scatter.5
  251.0 20.0 reduce-scatter.7
